TPU v7x, 32 devices: a whole 2x2x4 slice. The times are simulated.
32 devices in a mesh: grp: 2 (over y), sp: 4 (over z), tp: 4 (over x, core).
Axes of the slice: x: 2, y: 2, z: 4, core: 2. Of those that a mesh axis runs over, the one named last changes fastest.
Arguments:
- tokens: bfloat16 [2048, 2048], P(('grp', 'sp', 'tp')), parts along dimension 0, may hold values from -6 to 6
- norm_gain: float32 [2048], replicated, may hold values from 0.1 to 1.9
- conv_b_w: bfloat16 [2048, 1024], P('sp', 'tp'), may hold values from -0.125 to 0.125
- conv_c_w: bfloat16 [2048, 1024], P('sp', 'tp'), may hold values from -0.125 to 0.125
- conv_x_w: bfloat16 [2048, 1024], P('sp', 'tp'), may hold values from -0.125 to 0.125
- query_w: bfloat16 [2048, 1024], P('sp', 'tp'), may hold values from -1 to 1
- key_w: bfloat16 [2048, 256], P('sp', 'tp'), may hold values from -2 to 2
- value_w: bfloat16 [2048, 256], P('sp', 'tp'), may hold values from -0.125 to 0.125
- conv_taps: float32 [3, 1024], P(None, 'tp'), may hold values from -3.5 to 3.5
- gate_cache: float32 [2048, 16], P('grp', 'tp'), parts along dimension 0, as said below
- out_conv_w: bfloat16 [1024, 2048], P('tp'), may hold values from -0.1875 to 0.1875
- out_attn_w: bfloat16 [1024, 2048], P('tp'), may hold values from -0.75 to 0.75
Outputs:
- mixed: bfloat16 [2048, 2048], P(('grp', 'sp', 'tp')), parts along dimension 0
- log_total: float32 [2048, 16], P(('grp', 'sp'), 'tp'), parts along dimension 0
There are 2 independent parts, one for each index of `grp`. A program takes and returns all parts, laid end to end along the dimension named above; an argument that names none is the same for every part. Nothing has to cross between parts.
Inputs may be any that keep to these rules, and one draw needn't show every extreme that they name: `gate_cache`: never rises along positions; starts at or below zero.
All inputs are finite; a program needn't handle non-finite values.
Results may differ from a plain program's by a relative error of at most 0.017.
The roundings to bfloat16 on the way count: a program that leaves them out, or rounds other values in their place, can miss the bound.
Values may be sent and summed in bfloat16 or wider, within the bound.
A program may use at most 64 MiB of HBM per device.

v0:
```python
import jax
import jax.numpy as jnp
from jax import lax
from jax.sharding import PartitionSpec as P

HD = 64


def passed_along(value, axis, by):
    count = lax.axis_size(axis)
    pairs = [(i, i + by) for i in range(count) if 0 <= i + by < count]
    return lax.ppermute(value, axis, pairs)


def on_device(
    tokens,
    norm_gain,
    conv_b_w,
    conv_c_w,
    conv_x_w,
    query_w,
    key_w,
    value_w,
    conv_taps,
    gate_cache,
    out_conv_w,
    out_attn_w,
):
    rows = lax.all_gather(tokens, "tp", axis=0, tiled=True)
    count = rows.shape[0]
    xf = rows.astype(jnp.float32)
    scale_rows = lax.rsqrt(jnp.mean(xf * xf, axis=-1, keepdims=True) + 1e-05)
    normed = (xf * norm_gain).astype(jnp.bfloat16)

    def contract_all(pieces):
        width = pieces[0].shape[0]
        return tuple(
            (jnp.dot(normed, piece, preferred_element_type=jnp.float32) for piece in pieces)
        )

    conv_sums = contract_all(
        (
            lax.all_gather(conv_b_w, "sp", axis=0, tiled=True),
            lax.all_gather(conv_c_w, "sp", axis=0, tiled=True),
            lax.all_gather(conv_x_w, "sp", axis=0, tiled=True),
        )
    )
    attn_sums = contract_all(
        (
            lax.all_gather(query_w, "sp", axis=0, tiled=True),
            lax.all_gather(key_w, "sp", axis=0, tiled=True),
            lax.all_gather(value_w, "sp", axis=0, tiled=True),
        )
    )
    sums = conv_sums + attn_sums
    gate_b, gate_c, conv_in, query, key, value = [
        (total * scale_rows).astype(jnp.bfloat16) for total in sums
    ]
    taps = conv_taps.shape[0]
    channels = conv_in.shape[1]
    conv_src = (gate_c.astype(jnp.float32) * conv_in.astype(jnp.float32)).astype(jnp.bfloat16)
    earlier = passed_along(conv_src[count - (taps - 1) :], "sp", 1)
    padded = jnp.concatenate([earlier, conv_src], axis=0)
    filtered = jnp.zeros((count, channels), jnp.float32)
    for tap in range(taps):
        filtered = filtered + conv_taps[tap][None, :] * padded[tap : tap + count].astype(
            jnp.float32
        )
    conv_out = (gate_b.astype(jnp.float32) * filtered).astype(jnp.bfloat16)
    heads_dev = gate_cache.shape[1]
    kv_dev = key.shape[1] // HD
    group = heads_dev // kv_dev
    half = count // 2
    sp_index = lax.axis_index("sp")
    own_start = sp_index * count
    scale = HD ** (-0.5)
    later_query = query[half:]
    later_start = own_start + half

    def prepare(q_rows, begin):
        heads_q = q_rows.reshape(half, kv_dev, group, HD)
        q_gate = lax.dynamic_slice_in_dim(gate_cache, begin, half, 0).T.reshape(
            kv_dev, group, half, 1
        )
        q_pos = begin + jnp.arange(half, dtype=jnp.int32)
        return (heads_q, q_gate, q_pos)

    sides = (prepare(query[:half], own_start), prepare(later_query, later_start))

    def absorb(carry, side, key_rows, value_rows, begin):
        heads_q, q_gate, q_pos = side
        run_max, run_sum, acc = carry
        width = key_rows.shape[0]
        key_heads = key_rows.reshape(width, kv_dev, HD)
        value_heads = value_rows.reshape(width, kv_dev, HD)
        score = (
            jnp.einsum("qgjd,kgd->gjqk", heads_q, key_heads, preferred_element_type=jnp.float32)
            * scale
        )
        key_gate = lax.dynamic_slice_in_dim(gate_cache, begin, width, 0).T.reshape(
            kv_dev, group, 1, width
        )
        score = score + q_gate - key_gate
        mask = (begin + jnp.arange(width, dtype=jnp.int32))[None, :] <= q_pos[:, None]
        score = jnp.where(mask, score, -1e30)
        new_max = jnp.maximum(run_max, jnp.max(score, axis=-1))
        weight = jnp.where(mask, jnp.exp(score - new_max[..., None]), 0.0)
        factor = jnp.exp(run_max - new_max)
        new_sum = run_sum * factor + jnp.sum(weight, axis=-1)
        product = jnp.einsum(
            "gjqk,kgd->gjqd",
            weight.astype(jnp.bfloat16),
            value_heads,
            preferred_element_type=jnp.float32,
        )
        return (new_max, new_sum, acc * factor[..., None] + product)

    def guarded(carry, side, key_rows, value_rows, begin):

        def visit_rows(state):
            return absorb(state, side, key_rows, value_rows, begin)

        def keep(state):
            return state

        return lax.cond(begin <= side[2][half - 1], visit_rows, keep, carry)

    def absorb_both(carry, key_rows, value_rows, begin):
        return (
            guarded(carry[0], sides[0], key_rows, value_rows, begin),
            guarded(carry[1], sides[1], key_rows, value_rows, begin),
        )

    def fresh():
        return (
            jnp.full((kv_dev, group, half), -1e30, jnp.float32),
            jnp.zeros((kv_dev, group, half), jnp.float32),
            jnp.zeros((kv_dev, group, half, HD), jnp.float32),
        )

    key_rows = lax.all_gather(key, "sp", axis=0, tiled=True)
    value_rows = lax.all_gather(value, "sp", axis=0, tiled=True)
    width = key_rows.shape[0]
    step = 512
    key_blocks = key_rows.reshape(width // step, step, key_rows.shape[1])
    value_blocks = value_rows.reshape(width // step, step, value_rows.shape[1])
    firsts = step * jnp.arange(width // step, dtype=jnp.int32)

    def visit(state, inputs):
        return (absorb_both(state, inputs[0], inputs[1], inputs[2]), None)

    result, unused = lax.scan(visit, (fresh(), fresh()), (key_blocks, value_blocks, firsts))

    def finish(state):
        run_max, run_sum, acc = state
        out = (
            (acc / run_sum[..., None])
            .transpose(2, 0, 1, 3)
            .reshape(half, heads_dev * HD)
            .astype(jnp.bfloat16)
        )
        lse = (run_max + jnp.log(run_sum)).transpose(2, 0, 1).reshape(half, heads_dev)
        return (out, lse)

    early_out, early_lse = finish(result[0])
    later_out, later_lse = finish(result[1])
    attn_out = jnp.concatenate([early_out, later_out], axis=0)
    log_total = jnp.concatenate([early_lse, later_lse], axis=0)
    term = jnp.dot(conv_out, out_conv_w, preferred_element_type=jnp.float32)
    mixed = lax.psum_scatter(
        (term + jnp.dot(attn_out, out_attn_w, preferred_element_type=jnp.float32)).astype(
            jnp.bfloat16
        ),
        "tp",
        scatter_dimension=0,
        tiled=True,
    )
    return (mixed, log_total)


def solution(mesh):
    placed = (
        P(("grp", "sp", "tp"), None),
        P(),
        P("sp", "tp"),
        P("sp", "tp"),
        P("sp", "tp"),
        P("sp", "tp"),
        P("sp", "tp"),
        P("sp", "tp"),
        P(None, "tp"),
        P("grp", "tp"),
        P("tp", None),
        P("tp", None),
    )
    return jax.shard_map(
        on_device,
        mesh=mesh,
        in_specs=placed,
        out_specs=(P(("grp", "sp", "tp"), None), P(("grp", "sp"), "tp")),
        check_vma=False,
    )
```

profile of v0, /device:TPU:0, one launch (start us, length us, event | category | flops | bytes accessed | tf_op | source)
XLA Modules:
  0.0 184.9 jit_solution(1602423450954660975)
XLA Ops:
  7.2 0.0 copy-start
  7.2 0.0 copy-start.3
  7.2 0.0 all-gather.6.cloned.1.call-start
  7.2 0.7 all-gather.6.cloned.1.call-update
  7.9 0.0 all-gather.14.cloned.1.call-start
  8.0 0.7 all-gather.14.cloned.1.call-update
  8.7 0.0 all-gather.12.cloned.1.call-start
  8.7 0.7 all-gather.12.cloned.1.call-update
  9.4 0.0 all-gather.10.cloned.1.call-start
  9.5 0.5 all-gather.10.cloned.1.call-update
  10.0 0.0 all-gather.8.cloned.1.call-start
  10.0 0.5 all-gather.8.cloned.1.call-update
  10.6 0.0 reduce-scatter.2.cloned.1.call-start
  10.6 15.9 %all_gather.33 = bf16[2048,64]{0,1:T(8,128)(2,1)S(1)} all-gather(bf16[512,64]{0,1:T(8,128)(2,1)} %param.25), channel_id=1, replica_groups=mesh['grp'=2,'sp'=4,'tp'=4] {'sp'}, dimensions={0}, use_global_device_ids=true | all-gather | bytes 327680 | tf_op jit(solution)/shard_map/all_gather | solution.py:52
  26.5 15.1 %all_gather.31 = bf16[2048,64]{0,1:T(8,128)(2,1)S(1)} all-gather(bf16[512,64]{0,1:T(8,128)(2,1)} %param.24), channel_id=1, replica_groups=mesh['grp'=2,'sp'=4,'tp'=4] {'sp'}, dimensions={0}, use_global_device_ids=true | all-gather | bytes 327680 | tf_op jit(solution)/shard_map/all_gather | solution.py:51
  41.6 0.8 fusion.81
  42.4 0.7 dynamic-slice_bitcast_fusion.4
  43.1 1.6 fusion.36
  44.7 13.9 %all-gather.14.cloned.1.call-done = bf16[2048,256]{1,0:T(8,128)(2,1)} async-done(((bf16[512,256]{1,0:T(8,128)(2,1)}), bf16[2048,256]{1,0:T(8,128)(2,1)}) %all-gather.14.cloned.1.call-update) | async-done | bytes 1048592 | tf_op jit(solution)/shard_map/all_gather | solution.py:50
  58.6 0.0 copy-done.3
  58.6 2.0 %fusion.47 = bf16[256,256]{1,0:T(8,128)(2,1)S(1)} fusion(bf16[2048,256]{1,0:T(8,128)(2,1)} %all-gather.14.cloned.1.call-done, bf16[256,2048]{1,0:T(8,128)(2,1)} %all-gather.6.cloned.1.call-done, f32[2048]{0:T(1024)S(1)} %copy-done.3, f32[256]{0:T(256)S(1)} %add_rsqrt_fusion), kind=kOutput, calls=%fused_computation.72 | convolution fusion | flops 270139392 | bytes 2237440 | tf_op jit(solution)/shard_map/dot_general | solution.py:38
  60.6 0.1 copy.24
  60.7 0.1 copy.25
  60.8 0.0 copy-done.1
  60.9 0.5 fusion.50
  61.3 14.2 %all_gather.34 = bf16[1024,64]{0,1:T(8,128)(2,1)S(1)} all-gather(bf16[256,64]{0,1:T(8,128)(2,1)S(1)} %fusion.50), channel_id=1, replica_groups=mesh['grp'=2,'sp'=4,'tp'=4] {'sp'}, dimensions={0}, use_global_device_ids=true | all-gather | bytes 163840 | tf_op jit(solution)/shard_map/all_gather | solution.py:142
  75.5 0.5 fusion.49
  76.0 14.5 %all_gather.32 = bf16[1024,64]{0,1:T(8,128)(2,1)S(1)} all-gather(bf16[256,64]{0,1:T(8,128)(2,1)S(1)} %fusion.49), channel_id=1, replica_groups=mesh['grp'=2,'sp'=4,'tp'=4] {'sp'}, dimensions={0}, use_global_device_ids=true | all-gather | bytes 163840 | tf_op jit(solution)/shard_map/all_gather | solution.py:141
  90.5 0.4 all-gather.12.cloned.1.call-done
  90.9 1.7 fusion.46
  92.5 0.0 copy-start.2
  92.6 26.8 %all-gather.10.cloned.1.call-done = bf16[2048,256]{1,0:T(8,128)(2,1)} async-done(((bf16[512,256]{1,0:T(8,128)(2,1)}), bf16[2048,256]{1,0:T(8,128)(2,1)}) %all-gather.10.cloned.1.call-update) | async-done | bytes 1048592 | tf_op jit(solution)/shard_map/all_gather | solution.py:44
  119.4 1.7 fusion.44
  121.0 3.4 %collective-permute-start = (bf16[2,256]{1,0:T(2,128)(2,1)S(1)}, bf16[2,256]{1,0:T(2,128)(2,1)S(1)}, u32[]{:S(2)}, u32[]{:S(2)}) collective-permute-start(bf16[2,256]{1,0:T(2,128)(2,1)S(1)} %slice.38), channel_id=1, source_target_pairs={{0,4},{4,8},{8,12},{1,5},{5,9},{9,13},{2,6},{6,10},{10,14},{3,7},{... | collective-permute-start | bytes 3080 | tf_op jit(solution)/shard_map/ppermute | solution.py:12
  124.5 0.0 copy-done.2
  124.5 16.7 %while.20 = (s32[]{:T(128)}, f32[1,4,128]{2,1,0:T(4,128)S(1)}, f32[1,4,128]{2,1,0:T(4,128)S(1)}, f32[1,4,128,64]{2,3,1,0:T(8,128)S(1)}, f32[1,4,128]{2,1,0:T(4,1...) while((s32[]{:T(128)}, f32[1,4,128]{2,1,0:T(4,128)S(1)}, ...), condition=%wide.region_10.11_spmd, body=%wide.region_1.10_spmd.sunk | while | flops 140251136 | bytes 8123973 | solution.py:152
  124.5 0.6 dynamic_slice.34
  125.1 0.6 slice.61
  127.0 3.9 %conditional.5 = ((f32[1,4,128]{2,1,0:T(4,128)S(1)}, f32[1,4,128]{2,1,0:T(4,128)S(1)}, f32[1,4,128,64]{2,3,1,0:T(8,128)S(1)})) conditional(s32[]{:T(128)} %convert_element_type.190, (f32[1,4,128]{2,1,0:T(4,128)S(1)}, f32[1,4,128]{2,1,0:T(4,128)S(1)}, f32[1,4,128,64]{2,3,1,0:T(8,128)S(1)}) %tuple.56, (s32[]{:T(128)}, s32[128]{0:T(128)S(1)}, ...), branch_computations={%region_6.6_spmd, %region_7.9_spmd} | conditional | flops 70125568 | bytes 3930698 | solution.py:126
  129.0 0.1 dynamic-slice_bitcast_fusion.1
  129.1 0.6 iota_add_fusion.1
  129.7 0.1 broadcast_compare_fusion.1
  129.9 0.4 fusion.79
  130.3 0.3 fusion.21
  130.7 0.2 fusion.23
  130.9 0.6 slice.60
  132.8 3.9 %conditional.4 = ((f32[1,4,128]{2,1,0:T(4,128)S(1)}, f32[1,4,128]{2,1,0:T(4,128)S(1)}, f32[1,4,128,64]{2,3,1,0:T(8,128)S(1)})) conditional(s32[]{:T(128)} %convert_element_type.189, (f32[1,4,128]{2,1,0:T(4,128)S(1)}, f32[1,4,128]{2,1,0:T(4,128)S(1)}, f32[1,4,128,64]{2,3,1,0:T(8,128)S(1)}) %tuple.54, (s32[]{:T(128)}, s32[128]{0:T(128)S(1)}, ...), branch_computations={%region_2.2_spmd, %region_3.5_spmd} | conditional | flops 70125568 | bytes 3930698 | solution.py:126
  134.8 0.1 dynamic-slice_bitcast_fusion
  134.9 0.6 iota_add_fusion
  135.5 0.1 broadcast_compare_fusion
  135.7 0.4 fusion.78
  136.1 0.3 fusion.4
  136.4 0.2 fusion.6
  136.7 0.6 dynamic_slice.34
  137.3 0.6 slice.61
  139.3 0.6 slice.60
  141.3 6.8 %all-gather.8.cloned.1.call-done = bf16[2048,256]{1,0:T(8,128)(2,1)} async-done(((bf16[512,256]{1,0:T(8,128)(2,1)}), bf16[2048,256]{1,0:T(8,128)(2,1)}) %all-gather.8.cloned.1.call-update) | async-done | bytes 1048592 | tf_op jit(solution)/shard_map/all_gather | solution.py:43
  148.1 0.0 collective-permute-done
  148.1 0.0 copy-done
  148.1 2.8 %fusion.48 = f32[256,2048]{1,0:T(8,128)S(1)} fusion(bf16[256,2048]{1,0:T(8,128)(2,1)S(1)} %copy-done, bf16[2048,256]{1,0:T(8,128)(2,1)} %all-gather.8.cloned.1.call-done, bf16[256,2048]{1,0:T(8,128)(2,1)} %all-gather.6.cloned.1.call-done, f32[2048]{0:T(1024)S(1)} %copy-done.3, bf16[256,256]{1,0:T(8,128)(2,1)S(1)} %fusion.44, ...), kind=kOutput, calls=%fused_computation.73 | convolution fusion | flops 539688960 | bytes 5387264 | tf_op jit(solution)/shard_map/dot_general | solution.py:169
  150.9 2.7 %fusion.34 = bf16[256,2048]{1,0:T(8,128)(2,1)} fusion(f32[256,2048]{1,0:T(8,128)S(1)} %fusion.48, bf16[256,2048]{1,0:T(8,128)(2,1)} %param.29, bf16[128,256]{0,1:T(8,128)(2,1)S(1)} %bitcast.151, bf16[128,256]{0,1:T(8,128)(2,1)S(1)} %bitcast.150), kind=kOutput, calls=%fused_computation.55 | convolution fusion | flops 269746176 | bytes 4325376 | tf_op jit(solution)/shard_map/dot_general | solution.py:171
  153.6 0.0 reduce-scatter.2.cloned.1.call-update
  153.7 0.6 pad_maximum_fusion.2
  154.3 23.8 %reduce-scatter.2.cloned.1.call-done = bf16[64,2048]{1,0:T(8,128)(2,1)} async-done(((bf16[256,2048]{1,0:T(8,128)(2,1)}), bf16[64,2048]{1,0:T(8,128)(2,1)}) %reduce-scatter.2.cloned.1.call-update) | async-done | bytes 262160 | tf_op jit(solution)/shard_map/reduce_scatter | solution.py:170
  (29 shorter events, 0.3 us)
Async XLA Ops:
  7.2 140.9 %copy-start = (bf16[256,2048]{1,0:T(8,128)(2,1)S(1)}, bf16[256,2048]{1,0:T(8,128)(2,1)}, u32[]{:S(2)}) copy-start(bf16[256,2048]{1,0:T(8,128)(2,1)} %param.28) | copy-start | bytes 3145732
  7.2 51.4 %copy-start.3 = (f32[2048]{0:T(1024)S(1)}, f32[2048]{0:T(1024)}, u32[]{:S(2)}) copy-start(f32[2048]{0:T(1024)} %param.19) | copy-start | bytes 24580
  7.2 35.9 %all-gather.6.cloned.1.call-start = ((), (), s32[]{:S(2)}) async-start(), calls=%async_computation.1 | async-start | bytes 1310720 | tf_op jit(solution)/shard_map/all_gather | solution.py:29
  7.9 50.7 %all-gather.14.cloned.1.call-start = ((), (), s32[]{:S(2)}) async-start(), calls=%async_computation.5 | async-start | bytes 1310720 | tf_op jit(solution)/shard_map/all_gather | solution.py:50
  8.7 82.2 %all-gather.12.cloned.1.call-start = ((), (), s32[]{:S(2)}) async-start(), calls=%async_computation.4 | async-start | bytes 1310720 | tf_op jit(solution)/shard_map/all_gather | solution.py:45
  9.4 109.9 %all-gather.10.cloned.1.call-start = ((), (), s32[]{:S(2)}) async-start(), calls=%async_computation.3 | async-start | bytes 1310720 | tf_op jit(solution)/shard_map/all_gather | solution.py:44
  10.0 138.1 %all-gather.8.cloned.1.call-start = ((), (), s32[]{:S(2)}) async-start(), calls=%async_computation.2 | async-start | bytes 1310720 | tf_op jit(solution)/shard_map/all_gather | solution.py:43
  10.6 167.5 %reduce-scatter.2.cloned.1.call-start = ((), (), s32[]{:S(2)}) async-start(), calls=%async_computation.6 | async-start | bytes 1310720 | tf_op jit(solution)/shard_map/reduce_scatter | solution.py:170
  43.1 17.7 %copy-start.1 = (bf16[256,2048]{1,0:T(8,128)(2,1)S(1)}, bf16[256,2048]{1,0:T(8,128)(2,1)}, u32[]{:S(2)}) copy-start(bf16[256,2048]{1,0:T(8,128)(2,1)} %all-gather.6.cloned.1.call-done) | copy-start | bytes 3145732
  92.5 31.9 %copy-start.2 = (f32[1024,4]{0,1:T(4,128)S(1)}, f32[1024,4]{0,1:T(4,128)}, u32[]{:S(2)}) copy-start(f32[1024,4]{0,1:T(4,128)} %param.27) | copy-start | bytes 49156
  121.0 27.0 %collective-permute-start = (bf16[2,256]{1,0:T(2,128)(2,1)S(1)}, bf16[2,256]{1,0:T(2,128)(2,1)S(1)}, u32[]{:S(2)}, u32[]{:S(2)}) collective-permute-start(bf16[2,256]{1,0:T(2,128)(2,1)S(1)} %slice.38), channel_id=1, source_target_pairs={{0,4},{4,8},{8,12},{1,5},{5,9},{9,13},{2,6},{6,10},{10,14},{3,7},{... | collective-permute-start | bytes 3080 | tf_op jit(solution)/shard_map/ppermute | solution.py:12
Sparse Core Ops, SparseCore 0:
  9.6 19.4 all-gather.5
  30.6 27.9 all-gather.13
  60.2 30.6 all-gather.11
  92.3 27.0 all-gather.9
  120.8 27.2 all-gather.7
  153.8 24.2 reduce-scatter.1
where the time goes:
time: 186 us; the launch traced here: 185 us
  waiting for transfers between devices  74.8 us (40%)
  blocking collectives  59.7 us (32%)
  between operations  14.3 us (8%)
  matrix products  13.3 us (7%)
  loops' own time  9.22 us (5%)
  local copies, waits for them, and re-layouts  5.78 us (3%)
  other arithmetic  4.29 us (2%)
  starting transfers between devices  3.58 us (2%)
    all_gather x1, waiting for transfers between devices, on_device(): lax.all_gather(conv_c_w, 'sp', axis=0, tiled=True)  26.8 us
    reduce_scatter x1, waiting for transfers between devices, on_device(): lax.psum_scatter((term + jnp.dot(attn_out, out_attn_w, preferred_element_...  23.8 us
    all_gather x1, blocking collectives, on_device(): lax.all_gather(value_w, 'sp', axis=0, tiled=True)  15.9 us
    all_gather x1, blocking collectives, on_device(): lax.all_gather(key_w, 'sp', axis=0, tiled=True)  15.1 us
    all_gather x1, blocking collectives, on_device(): key_rows = lax.all_gather(key, 'sp', axis=0, tiled=True)  14.5 us
    all_gather x1, blocking collectives, on_device(): value_rows = lax.all_gather(value, 'sp', axis=0, tiled=True)  14.2 us
    all_gather x1, waiting for transfers between devices, on_device(): lax.all_gather(query_w, 'sp', axis=0, tiled=True)  13.9 us
    all_gather x1, waiting for transfers between devices, on_device(): lax.all_gather(conv_b_w, 'sp', axis=0, tiled=True)  6.81 us
  transfers between devices with their start and end apart: 7, of which 5 were waited for; matrix products, arithmetic and copies ran while one was open for 10% of the time, Pallas kernels for 0%

commit v1 on v0

--- a/solution.py
+++ b/solution.py
@@ -1,9 +1,345 @@
+import functools
+
 import jax
 import jax.numpy as jnp
 from jax import lax
+from jax.experimental import pallas as pl
+from jax.experimental.pallas import tpu as pltpu
 from jax.sharding import PartitionSpec as P
 
 HD = 64
+LANES = 128
+MESH = pl.DeviceIdType.MESH
+F32 = jnp.float32
+BF16 = jnp.bfloat16
+
+
+def layer_kernel(
+    n_sp,
+    n_tp,
+    tokens_ref,
+    gain_ref,
+    wb_ref,
+    wc_ref,
+    wx_ref,
+    wq_ref,
+    wk_ref,
+    wv_ref,
+    taps_ref,
+    gate_ref,
+    oconv_ref,
+    oattn_ref,
+    mixed_ref,
+    lse_ref,
+    tok,
+    normed,
+    wconv,
+    wq,
+    wkv,
+    kvall,
+    csrc,
+    halo,
+    comb,
+    wout,
+    part,
+    sib,
+    fwd,
+    xin,
+    send_sem,
+    recv_sem,
+    local_sem,
+):
+    g = lax.axis_index("grp")
+    s = lax.axis_index("sp")
+    t = lax.axis_index("tp")
+    up = {"sp": lax.rem(s + 1, n_sp)}
+    down = {"sp": lax.rem(s + n_sp - 1, n_sp)}
+    across = {"grp": 1 - g}
+    depth = wb_ref.shape[0]
+    rows_own = tokens_ref.shape[0]
+    count = tok.shape[0]
+    conv_w = (wb_ref, wc_ref, wx_ref)
+    heads = wq_ref.shape[1] // HD
+    channels = wb_ref.shape[1]
+
+    def block(index, size):
+        return pl.ds(pl.multiple_of(index * size, size), size)
+
+    def shard(by):
+        return block(lax.rem(s + by + n_sp, n_sp), depth)
+
+    local = [
+        pltpu.make_async_copy(oconv_ref, wout.at[pl.ds(0, channels)], local_sem.at[0]),
+        pltpu.make_async_copy(
+            oattn_ref, wout.at[pl.ds(channels, heads * HD)], local_sem.at[1]
+        ),
+    ]
+    for copy in local:
+        copy.start()
+    wkv[shard(0), :] = jnp.concatenate([wk_ref[...], wv_ref[...]], axis=1)
+
+    barrier = pltpu.get_barrier_semaphore()
+    for by in range(1, n_sp):
+        pl.semaphore_signal(
+            barrier, inc=1, device_id={"sp": lax.rem(s + by, n_sp)}, device_id_type=MESH
+        )
+    for by in range(1, n_tp):
+        pl.semaphore_signal(
+            barrier, inc=1, device_id={"tp": lax.rem(t + by, n_tp)}, device_id_type=MESH
+        )
+    pl.semaphore_signal(barrier, inc=1, device_id=across, device_id_type=MESH)
+    pl.semaphore_wait(barrier, n_sp + n_tp - 1)
+
+    sent = []
+    used = [0]
+
+    def send(src, dst, device):
+        index = used[0]
+        used[0] += 1
+        copy = pltpu.make_async_remote_copy(
+            src_ref=src,
+            dst_ref=dst,
+            send_sem=send_sem.at[index],
+            recv_sem=recv_sem.at[index],
+            device_id=device,
+            device_id_type=MESH,
+        )
+        copy.start()
+        sent.append(copy)
+        return copy
+
+    def conv_piece(m, by):
+        return wconv.at[m, g, shard(by)]
+
+    plus_x, minus_x = [], []
+    for m in range(3):
+        src = conv_w[m].at[:, block(g, LANES)]
+        plus_x.append(send(src, conv_piece(m, 0), up))
+        minus_x.append(send(src, conv_piece(m, 0), down))
+    own_kv, own_q = wkv.at[shard(0)], wq.at[shard(0)]
+    plus_kv = send(own_kv, own_kv, up)
+    minus_kv = send(own_kv, own_kv, down)
+    plus_q = send(wq_ref, own_q, up)
+    minus_q = send(wq_ref, own_q, down)
+    token_copies = [
+        send(tokens_ref, tok.at[block(t, rows_own)], {"tp": lax.rem(t + by, n_tp)})
+        for by in range(1, n_tp)
+    ]
+    tok[block(t, rows_own), :] = tokens_ref[...]
+    for m in range(3):
+        for h in range(2):
+            wconv[m, h, shard(0), :] = conv_w[m][:, h * LANES : (h + 1) * LANES]
+    wq[shard(0), :] = wq_ref[...]
+    padding = jnp.zeros((gate_ref.shape[0], LANES - heads), F32)
+    gate_rows = jnp.concatenate([gate_ref[...], padding], axis=1).T[:heads]
+
+    over_y, hop_x = [], []
+    for m in range(3):
+        plus_x[m].wait_recv()
+        over_y.append(send(conv_piece(m, -1), conv_piece(m, -1), across))
+        hop_x.append(send(conv_piece(m, -1), conv_piece(m, -1), up))
+        minus_x[m].wait_recv()
+        over_y.append(send(conv_piece(m, 1), conv_piece(m, 1), across))
+
+    for copy in token_copies:
+        copy.wait_recv()
+    square = jnp.zeros((count, 1), F32)
+    width = tok.shape[1]
+    step = width // 4
+    for c in range(4):
+        cols = slice(c * step, (c + 1) * step)
+        xf = tok[:, cols].astype(F32)
+        square = square + jnp.sum(xf * xf, axis=-1, keepdims=True)
+        normed[:, cols] = (xf * gain_ref[:, cols]).astype(BF16)
+    scale_rows = lax.rsqrt(square / width + 1e-05)
+
+    def project(weight):
+        return (
+            jnp.dot(normed[...], weight, preferred_element_type=F32) * scale_rows
+        ).astype(BF16)
+
+    plus_kv.wait_recv()
+    minus_kv.wait_recv()
+    hop_kv = send(wkv.at[shard(1)], wkv.at[shard(1)], down)
+    plus_q.wait_recv()
+    minus_q.wait_recv()
+    hop_q = send(wq.at[shard(1)], wq.at[shard(1)], down)
+    hop_x[0].wait_recv()
+    over_y.append(send(conv_piece(0, -2), conv_piece(0, -2), across))
+    hop_kv.wait_recv()
+    own_rows = block(s, count)
+    kvall[own_rows, :] = project(wkv[...])
+    kv_copies = [
+        send(kvall.at[own_rows], kvall.at[own_rows], {"sp": lax.rem(s + by, n_sp)})
+        for by in range(1, n_sp)
+    ]
+    for m in range(1, 3):
+        hop_x[m].wait_recv()
+        over_y.append(send(conv_piece(m, -2), conv_piece(m, -2), across))
+
+    hop_q.wait_recv()
+    query = project(wq[...]) * BF16(HD**-0.5)
+    for copy in kv_copies:
+        copy.wait_recv()
+    keys = kvall[:, :HD]
+    values = kvall[:, HD:]
+    total_keys = kvall.shape[0]
+    q_pos = s * count + lax.broadcasted_iota(jnp.int32, (count, total_keys), 0)
+    visible = lax.broadcasted_iota(jnp.int32, (count, total_keys), 1) <= q_pos
+    for h in range(heads):
+        score = lax.dot_general(
+            query[:, h * HD : (h + 1) * HD],
+            keys,
+            (((1,), (1,)), ((), ())),
+            preferred_element_type=F32,
+        )
+        score = score + gate_ref[own_rows, h : h + 1] - gate_rows[h : h + 1]
+        score = jnp.where(visible, score, -1e30)
+        row_max = jnp.max(score, axis=-1, keepdims=True)
+        weight = jnp.exp(score - row_max)
+        row_sum = jnp.sum(weight, axis=-1, keepdims=True)
+        out = jnp.dot(weight.astype(BF16), values, preferred_element_type=F32)
+        comb[:, channels + h * HD : channels + (h + 1) * HD] = (out / row_sum).astype(BF16)
+        lse_ref[:, h : h + 1] = row_max + jnp.log(row_sum)
+
+    for copy in over_y:
+        copy.wait_recv()
+    gates = []
+    tail = halo.shape[0]
+    for h in range(2):
+        cols = slice(h * LANES, (h + 1) * LANES)
+        gates.append(project(wconv[0, h]))
+        gate_c = project(wconv[1, h]).astype(F32)
+        csrc[:, cols] = (gate_c * project(wconv[2, h]).astype(F32)).astype(BF16)
+    halo_copy = send(csrc.at[pl.ds(count - tail, tail)], halo, up)
+    halo_copy.wait_recv()
+    taps = taps_ref.shape[0]
+    before = jnp.where(s > 0, halo[...].astype(F32), 0.0)
+    source = csrc[...].astype(F32)
+    filtered = jnp.zeros((count, channels), F32)
+    for tap in range(taps):
+        back = taps - 1 - tap
+        moved = source
+        if back:
+            moved = jnp.concatenate([before[tail - back :], source[: count - back]], axis=0)
+        filtered = filtered + taps_ref[tap : tap + 1, :] * moved
+    for h in range(2):
+        cols = slice(h * LANES, (h + 1) * LANES)
+        comb[:, cols] = (gates[h].astype(F32) * filtered[:, cols]).astype(BF16)
+
+    for copy in local:
+        copy.wait()
+    sibling = t + 1 - 2 * lax.rem(t, 2)
+    far = lax.rem(t + 2, n_tp)
+    far_sibling = lax.rem(sibling + 2, n_tp)
+    chunks = 4
+    wide = width // chunks
+    near_copies, far_copies = [], []
+
+    def relay(c):
+        cols = pl.ds(c * wide, wide)
+        for copy in near_copies[c]:
+            copy.wait_recv()
+        pair = part[far, :, cols].astype(F32) + sib[1, :, cols].astype(F32)
+        fwd[:, cols] = pair.astype(BF16)
+        far_copies.append(send(fwd.at[:, cols], xin.at[:, cols], {"tp": far}))
+
+    for c in range(chunks):
+        cols = pl.ds(c * wide, wide)
+        term = jnp.dot(comb[...], wout[:, cols], preferred_element_type=F32).astype(BF16)
+        for j in range(n_tp):
+            part[j, :, cols] = term[j * rows_own : (j + 1) * rows_own]
+        near_copies.append(
+            [
+                send(part.at[far_sibling, :, cols], sib.at[1, :, cols], {"tp": sibling}),
+                send(part.at[sibling, :, cols], sib.at[0, :, cols], {"tp": sibling}),
+            ]
+        )
+        if c:
+            relay(c - 1)
+    relay(chunks - 1)
+    for c in range(chunks):
+        cols = pl.ds(c * wide, wide)
+        far_copies[c].wait_recv()
+        whole = part[t, :, cols].astype(F32) + sib[0, :, cols].astype(F32)
+        mixed_ref[:, cols] = (whole + xin[:, cols].astype(F32)).astype(BF16)
+    for copy in sent:
+        copy.wait_send()
+
+
+COPIES = 64
+
+
+def in_one_kernel(
+    n_sp,
+    n_tp,
+    tokens,
+    norm_gain,
+    conv_b_w,
+    conv_c_w,
+    conv_x_w,
+    query_w,
+    key_w,
+    value_w,
+    conv_taps,
+    gate_cache,
+    out_conv_w,
+    out_attn_w,
+):
+    rows, width = tokens.shape
+    count = rows * n_tp
+    depth, channels = conv_b_w.shape
+    q_width = query_w.shape[1]
+    heads = gate_cache.shape[1]
+    kv_width = key_w.shape[1] + value_w.shape[1]
+    total = gate_cache.shape[0]
+    vmem = pl.BlockSpec(memory_space=pltpu.VMEM)
+    hbm = pl.BlockSpec(memory_space=pl.ANY)
+    out_rows = out_conv_w.shape[0] + out_attn_w.shape[0]
+    return pl.pallas_call(
+        functools.partial(layer_kernel, n_sp, n_tp),
+        out_shape=(
+            jax.ShapeDtypeStruct((rows, width), BF16),
+            jax.ShapeDtypeStruct((count, heads), F32),
+        ),
+        in_specs=[vmem] * 10 + [hbm] * 2,
+        out_specs=(vmem, vmem),
+        scratch_shapes=[
+            pltpu.VMEM((count, width), BF16),
+            pltpu.VMEM((count, width), BF16),
+            pltpu.VMEM((3, channels // LANES, width, LANES), BF16),
+            pltpu.VMEM((width, q_width), BF16),
+            pltpu.VMEM((width, kv_width), BF16),
+            pltpu.VMEM((total, kv_width), BF16),
+            pltpu.VMEM((count, channels), BF16),
+            pltpu.VMEM((16, channels), BF16),
+            pltpu.VMEM((count, channels + q_width), BF16),
+            pltpu.VMEM((out_rows, width), BF16),
+            pltpu.VMEM((n_tp, rows, width), BF16),
+            pltpu.VMEM((2, rows, width), BF16),
+            pltpu.VMEM((rows, width), BF16),
+            pltpu.VMEM((rows, width), BF16),
+            pltpu.SemaphoreType.DMA((COPIES,)),
+            pltpu.SemaphoreType.DMA((COPIES,)),
+            pltpu.SemaphoreType.DMA((2,)),
+        ],
+        compiler_params=pltpu.CompilerParams(
+            collective_id=0, has_side_effects=True, vmem_limit_bytes=56 * 1024 * 1024
+        ),
+    )(
+        tokens,
+        norm_gain.reshape(1, width),
+        conv_b_w,
+        conv_c_w,
+        conv_x_w,
+        query_w,
+        key_w,
+        value_w,
+        conv_taps,
+        gate_cache,
+        out_conv_w,
+        out_attn_w,
+    )
 
 
 def passed_along(value, axis, by):
@@ -193,8 +529,17 @@
         P("tp", None),
         P("tp", None),
     )
+    sizes = dict(mesh.shape)
+
+    def on_one(*args):
+        channels, key_width = args[2].shape[1], args[6].shape[1]
+        grid = (sizes["grp"], sizes["sp"], sizes["tp"])
+        if grid == (2, 4, 4) and channels == 2 * LANES and key_width == HD:
+            return in_one_kernel(sizes["sp"], sizes["tp"], *args)
+        return on_device(*args)
+
     return jax.shard_map(
-        on_device,
+        on_one,
         mesh=mesh,
         in_specs=placed,
         out_specs=(P(("grp", "sp", "tp"), None), P(("grp", "sp"), "tp")),

time: 186 us -> 92 us (0.49)
  Pallas kernels: 0 us -> 84.4 us
  waiting for transfers between devices: 74.8 us -> 0 us
  blocking collectives: 59.7 us -> 0 us
  between operations: 14.3 us -> 0.65 us
  matrix products: 13.3 us -> 0 us
  loops' own time: 9.22 us -> 0 us
  other arithmetic: 4.29 us -> 0 us
  starting transfers between devices: 3.58 us -> 0 us
    pallas_call x0 -> x1, Pallas kernels: none -> 84.4 us  [in_one_kernel(): pl.pallas_call(functools.partial(layer_kernel, n_sp, n_tp), out_shape=(ja...]
    all_gather x4 -> x0, blocking collectives: 59.7 us -> none  [the longest x1 15.9 us: on_device(): lax.all_gather(value_w, 'sp', axis=0, tiled=True)]
    all_gather x5 -> x0, waiting for transfers between devices: 47.9 us -> none  [the longest x1 26.8 us: on_device(): lax.all_gather(conv_c_w, 'sp', axis=0, tiled=True)]
    reduce_scatter x1 -> x0, waiting for transfers between devices: 23.8 us -> none  [on_device(): lax.psum_scatter((term + jnp.dot(attn_out, out_attn_w, preferred_element_...]
    dot_general x11 -> x0, matrix products: 13.3 us -> none  [the longest x5 6.21 us: contract_all(): jnp.dot(normed, piece, preferred_element_type=jnp.float32)]
    another operation x5 -> x0, loops' own time: 9.22 us -> none  [the longest x1 5.19 us: on_device(): lax.scan(visit, (fresh(), fresh()), (key_blocks, value_blocks, firsts))]
    unnamed x8, local copies, waits for them, and re-layouts: 0.02 us -> 5.08 us
    slice x9 -> x0, local copies, waits for them, and re-layouts: 3.63 us -> none  [the longest x4 2.58 us: guarded(): return lax.cond(begin <= side[2][half - 1], visit_rows, keep, carry)]
  transfers between devices with their start and end apart: 7 -> 0, of which waited for: 5 -> 0; matrix products, arithmetic and copies ran while one was open for 10% -> 0% of each run, Pallas kernels for 0% -> 0%
where the time goes in v1:
time: 92 us; the launch traced here: 91.7 us
  Pallas kernels  84.4 us (92%)
  local copies, waits for them, and re-layouts  6.66 us (7%)
    pallas_call x1, Pallas kernels, in_one_kernel(): pl.pallas_call(functools.partial(layer_kernel, n_sp, n_tp), out_shape=(ja...  84.4 us
    unnamed x8, local copies, waits for them, and re-layouts  5.08 us

profile of v1, /device:TPU:0, one launch (start us, length us, event | category | flops | bytes accessed | tf_op | source)
XLA Modules:
  0.0 91.7 jit_solution(17845346493555512361)
XLA Ops:
  0.6 0.0 copy-start
  0.6 1.6 %copy.14.wk_ref = bf16[512,64]{1,0:T(8,128)(2,1)} copy(bf16[512,64]{0,1:T(8,128)(2,1)} %param.18) | data formatting | bytes 131072 | tf_op args[6]
  2.3 0.0 copy-done
  2.3 0.0 copy-start.1
  2.3 0.8 copy.15.wv_ref
  3.0 0.0 copy-done.1
  3.0 1.0 %copy.16.gate_ref = f32[1024,4]{1,0:T(8,128)} copy(f32[1024,4]{0,1:T(4,128)S(1)} %copy-done.1) | data formatting | bytes 32768 | tf_op args[9]
  4.1 84.4 %shard_map.131 = (bf16[64,2048]{1,0:T(8,128)(2,1)}, f32[256,4]{1,0:T(8,128)}) custom-call(bf16[64,2048]{1,0:T(8,128)(2,1)} %tokens_ref.1, f32[1,2048]{1,0:T(1,128)} %bitcast.1, bf16[512,256]{1,0:T(8,128)(2,1)} %wb_ref.1, bf16[512,256]{1,0:T(8,128)(2,1)} %wc_ref.1, bf16[512,256]{1,0:T(8,128)(2,1)} %wx_ref.1, bf16[512,256]{1,0:T(8,128)(2,1)} %wq_ref.1, ...), custom_call_target="tpu_custom_call" | custom-call | tf_op jit(solution)/shard_map/pallas_call | solution.py:299
  88.5 1.6 %copy.17 = f32[256,4]{0,1:T(4,128)} copy(f32[256,4]{1,0:T(8,128)} %get-tuple-element.3) | data formatting | bytes 8192 | tf_op jit(solution)/shard_map/pallas_call | solution.py:299
  90.0 1.7 %copy.19 = bf16[64,2048]{1,0:T(8,128)(2,1)} copy(bf16[64,2048]{1,0:T(8,128)(2,1)} %get-tuple-element.6) | data formatting | bytes 524288
Async XLA Ops:
  0.6 1.6 %copy-start = (bf16[512,64]{0,1:T(8,128)(2,1)S(1)}, bf16[512,64]{0,1:T(8,128)(2,1)}, u32[]{:S(2)}) copy-start(bf16[512,64]{0,1:T(8,128)(2,1)} %param.19) | copy-start | bytes 196612
  2.3 0.8 copy-start.1

commit v2 on v0

--- a/solution.py
+++ b/solution.py
@@ -1,9 +1,403 @@
+import functools
+
 import jax
 import jax.numpy as jnp
 from jax import lax
+from jax.experimental import pallas as pl
+from jax.experimental.pallas import tpu as pltpu
 from jax.sharding import PartitionSpec as P
 
 HD = 64
+LANES = 128
+MESH = pl.DeviceIdType.MESH
+F32 = jnp.float32
+BF16 = jnp.bfloat16
+
+
+def layer_kernel(
+    n_sp,
+    n_tp,
+    tokens_ref,
+    gain_ref,
+    wb_ref,
+    wc_ref,
+    wx_ref,
+    wq_ref,
+    wk_ref,
+    wv_ref,
+    taps_ref,
+    gate_ref,
+    oconv_ref,
+    oattn_ref,
+    mixed_ref,
+    lse_ref,
+    tok,
+    normed,
+    packed,
+    wmain,
+    wkv,
+    proj,
+    outs,
+    comb,
+    lse_out,
+    lse_in,
+    wout,
+    part,
+    sib,
+    fwd,
+    xin,
+    send_sem,
+    tok_sem,
+    main_sem,
+    kv_sem,
+    out_sem,
+    sum_sem,
+    local_sem,
+):
+    g = lax.axis_index("grp")
+    s = lax.axis_index("sp")
+    t = lax.axis_index("tp")
+    across = {"grp": 1 - g}
+    sibling = t + 1 - 2 * lax.rem(t, 2)
+    far = lax.rem(t + 2, n_tp)
+    far_sibling = lax.rem(sibling + 2, n_tp)
+    depth = wb_ref.shape[0]
+    half = depth // 2
+    rows_own, width = tokens_ref.shape
+    count = rows_own * n_tp
+    total = count * n_sp
+    ch = wb_ref.shape[1] // n_sp
+
+    def block(index, size):
+        return pl.ds(pl.multiple_of(index * size, size), size)
+
+    local = []
+    for d in range(n_sp):
+        for k, ref in ((0, oconv_ref), (1, oattn_ref)):
+            local.append(
+                pltpu.make_async_copy(
+                    ref.at[pl.ds(d * ch, ch)],
+                    wout.at[pl.ds((2 * d + k) * ch, ch)],
+                    local_sem.at[2 * d + k],
+                )
+            )
+    for copy in local:
+        copy.start()
+
+    barrier = pltpu.get_barrier_semaphore()
+    for by in range(1, n_sp):
+        pl.semaphore_signal(
+            barrier, inc=1, device_id={"sp": lax.rem(s + by, n_sp)}, device_id_type=MESH
+        )
+    for by in range(1, n_tp):
+        pl.semaphore_signal(
+            barrier, inc=1, device_id={"tp": lax.rem(t + by, n_tp)}, device_id_type=MESH
+        )
+    pl.semaphore_signal(barrier, inc=1, device_id=across, device_id_type=MESH)
+    pl.semaphore_wait(barrier, n_sp + n_tp - 1)
+
+    used = [0]
+    sent = []
+
+    def send(src, dst, arrival, device, when=None):
+        index = used[0]
+        used[0] += 1
+        copy = pltpu.make_async_remote_copy(
+            src_ref=src,
+            dst_ref=dst,
+            send_sem=send_sem.at[index],
+            recv_sem=arrival,
+            device_id=device,
+            device_id_type=MESH,
+        )
+        sent.append((copy, when))
+        if when is None:
+            copy.start()
+        else:
+            pl.when(when)(copy.start)
+        return copy
+
+    def arrived(ref, arrival):
+        pltpu.make_async_remote_copy(
+            src_ref=ref,
+            dst_ref=ref,
+            send_sem=send_sem.at[0],
+            recv_sem=arrival,
+            device_id=across,
+            device_id_type=MESH,
+        ).wait_recv()
+
+    def both(a, b):
+        return b if a is None else jnp.logical_and(a, b)
+
+    def tok_block(z, x):
+        return tok.at[block(z * n_tp + x, rows_own)]
+
+    def tok_spread(src, z, step, when):
+        arrival = tok_sem.at[z * n_tp + t]
+        dst = tok_block(z, t)
+        if step >= 0:
+            send(src, dst, arrival, {"sp": lax.rem(s + 1, n_sp)}, both(when, s < n_sp - 1))
+        if step <= 0:
+            send(src, dst, arrival, {"sp": lax.rem(s + n_sp - 1, n_sp)}, both(when, s > 0))
+        send(src, dst, arrival, {"tp": far}, when)
+        send(src, dst, arrival, {"tp": sibling}, when)
+
+    def tok_round(h):
+        for step in (1, -1):
+            z = lax.rem(s - step * h + n_sp, n_sp)
+            exists = (s >= h) if step > 0 else (s + h < n_sp)
+
+            @pl.when(exists)
+            def _(z=z):
+                arrived(tok_block(z, t), tok_sem.at[z * n_tp + t])
+
+            tok_spread(tok_block(z, t), z, step, exists)
+
+    def tok_far(z):
+        arrival = tok_sem.at[z * n_tp + far]
+        arrived(tok_block(z, far), arrival)
+        send(tok_block(z, far), tok_block(z, far), arrival, {"tp": sibling})
+
+    def main_rows(z, g_half):
+        return wmain.at[block(2 * z + g_half, half)]
+
+    def kv_rows(z, g_half):
+        return wkv.at[block(2 * z + g_half, half)]
+
+    def weights_over(by):
+        z = lax.rem(s + by, n_sp)
+        arrived(main_rows(z, g), main_sem.at[z])
+        send(main_rows(z, g), main_rows(z, g), main_sem.at[n_sp + z], across)
+        arrived(kv_rows(z, g), kv_sem.at[z])
+        send(kv_rows(z, g), kv_rows(z, g), kv_sem.at[n_sp + z], across)
+
+    tok_spread(tokens_ref, s, 0, None)
+    tok[block(s * n_tp + t, rows_own), :] = tokens_ref[...]
+    for d in range(n_sp):
+        cols = slice(d * ch, (d + 1) * ch)
+        packed[d, :, : 2 * ch] = jnp.concatenate([wb_ref[:, cols], wc_ref[:, cols]], axis=1)
+        packed[d, :, 2 * ch :] = jnp.concatenate([wx_ref[:, cols], wq_ref[:, cols]], axis=1)
+    stacked = jnp.concatenate([wk_ref[...], wv_ref[...]], axis=0).astype(F32)
+    wkv[block(s, depth), :] = stacked.T.astype(BF16)
+    wmain[block(s, depth), :] = packed[s]
+
+    tok_round(1)
+    for by in (2, 1, 3):
+        d = lax.rem(s + by, n_sp)
+        send(packed.at[d, block(g, half)], main_rows(s, g), main_sem.at[s], {"sp": d})
+        send(kv_rows(s, g), kv_rows(s, g), kv_sem.at[s], {"sp": d})
+    tok_far(s)
+    tok_round(2)
+    for z_by in (1, 3):
+        weights_over(z_by)
+    tok_round(3)
+    weights_over(2)
+    for by in (1, 3, 2):
+        tok_far(lax.rem(s + by, n_sp))
+    for by in range(n_sp):
+        z = lax.rem(s + by, n_sp)
+        arrived(tok_block(z, sibling), tok_sem.at[z * n_tp + sibling])
+        arrived(tok_block(z, far_sibling), tok_sem.at[z * n_tp + far_sibling])
+
+    def normalize(i, unused):
+        rows = block(i, rows_own)
+        xf = tok[rows, :].astype(F32)
+        square = jnp.sum(xf * xf, axis=-1, keepdims=True)
+        normed[rows, :] = (xf * gain_ref[...]).astype(BF16)
+        scale = lax.rsqrt(square / width + 1e-05)
+        proj[rows, :] = jnp.broadcast_to(scale, (rows_own, proj.shape[1]))
+        return unused
+
+    lax.fori_loop(0, n_sp * n_tp, normalize, 0)
+    scale_rows = proj[:, :1]
+    gate_row = gate_ref[pl.ds(s, 1), :]
+    gate_column = jnp.broadcast_to(gate_row, (LANES, total)).T[:, :1]
+    taps = taps_ref.shape[0]
+    taps_own = jnp.zeros((taps, ch), F32)
+    for d in range(n_sp):
+        taps_own = jnp.where(s == d, taps_ref[:, d * ch : (d + 1) * ch], taps_own)
+
+    for by in range(1, n_sp):
+        z = lax.rem(s + by, n_sp)
+        arrived(main_rows(z, 1 - g), main_sem.at[n_sp + z])
+        arrived(kv_rows(z, 1 - g), kv_sem.at[n_sp + z])
+
+    def project(weight):
+        return (
+            jnp.dot(normed[...], weight, preferred_element_type=F32) * scale_rows
+        ).astype(BF16)
+
+    main = project(wmain[...])
+    kv = project(wkv[...])
+    gate_b = main[:, :ch].astype(F32)
+    conv_src = main[:, ch : 2 * ch].astype(F32) * main[:, 2 * ch : 3 * ch].astype(F32)
+    conv_src = conv_src.astype(BF16).astype(F32)
+    filtered = jnp.zeros((total, ch), F32)
+    for tap in range(taps):
+        back = taps - 1 - tap
+        moved = conv_src
+        if back:
+            moved = jnp.concatenate([jnp.zeros((back, ch), F32), conv_src[: total - back]], axis=0)
+        filtered = filtered + taps_own[tap : tap + 1] * moved
+    conv_out = (gate_b * filtered).astype(BF16)
+    query = main[:, 3 * ch :] * BF16(HD**-0.5)
+    keys, values = kv[:, :HD], kv[:, HD:]
+    for d in reversed(range(n_sp)):
+        rows = slice(d * count, (d + 1) * count)
+        seen = (d + 1) * count
+        score = lax.dot_general(
+            query[rows],
+            keys[:seen],
+            (((1,), (1,)), ((), ())),
+            preferred_element_type=F32,
+        )
+        score = score + gate_column[rows] - gate_row[:, :seen]
+        q_pos = d * count + lax.broadcasted_iota(jnp.int32, (count, seen), 0)
+        visible = lax.broadcasted_iota(jnp.int32, (count, seen), 1) <= q_pos
+        score = jnp.where(visible, score, -1e30)
+        row_max = jnp.max(score, axis=-1, keepdims=True)
+        weight = jnp.exp(score - row_max)
+        row_sum = jnp.sum(weight, axis=-1, keepdims=True)
+        out = jnp.dot(weight.astype(BF16), values[:seen], preferred_element_type=F32)
+        attn_out = (out / row_sum).astype(BF16)
+        outs[d] = jnp.concatenate([conv_out[rows], attn_out], axis=1)
+        logs = jnp.broadcast_to(row_max + jnp.log(row_sum), (count, LANES)).T
+        lse_out[d] = logs[: lse_out.shape[1]]
+        other = s != d
+        send(outs.at[d], comb.at[s], out_sem.at[s], {"sp": d}, other)
+        send(lse_out.at[d], lse_in.at[s], out_sem.at[n_sp + s], {"sp": d}, other)
+    comb[s] = outs[s]
+    lse_in[s] = lse_out[s]
+    for copy in local:
+        copy.wait()
+    for by in range(1, n_sp):
+        z = lax.rem(s + by, n_sp)
+        arrived(comb.at[z], out_sem.at[z])
+        arrived(lse_in.at[z], out_sem.at[n_sp + z])
+    for d in range(n_sp):
+        lse_ref[d : d + 1, :] = lse_in[d, :1]
+
+    gathered = jnp.concatenate([comb[d] for d in range(n_sp)], axis=1)
+    chunks = 4
+    wide = width // chunks
+
+    def relay(c):
+        cols = pl.ds(c * wide, wide)
+        for k in range(2):
+            arrived(sib.at[k, :, cols], sum_sem.at[3 * c + k])
+        pair = part[far, :, cols].astype(F32) + sib[1, :, cols].astype(F32)
+        fwd[:, cols] = pair.astype(BF16)
+        send(fwd.at[:, cols], xin.at[:, cols], sum_sem.at[3 * c + 2], {"tp": far})
+
+    for c in range(chunks):
+        cols = pl.ds(c * wide, wide)
+        term = jnp.dot(gathered, wout[:, cols], preferred_element_type=F32).astype(BF16)
+        for j in range(n_tp):
+            part[j, :, cols] = term[j * rows_own : (j + 1) * rows_own]
+        for k, owner in ((1, far_sibling), (0, sibling)):
+            send(
+                part.at[owner, :, cols],
+                sib.at[k, :, cols],
+                sum_sem.at[3 * c + k],
+                {"tp": sibling},
+            )
+        if c:
+            relay(c - 1)
+    relay(chunks - 1)
+    for c in range(chunks):
+        cols = pl.ds(c * wide, wide)
+        arrived(xin.at[:, cols], sum_sem.at[3 * c + 2])
+        whole = part[t, :, cols].astype(F32) + sib[0, :, cols].astype(F32)
+        mixed_ref[:, cols] = (whole + xin[:, cols].astype(F32)).astype(BF16)
+    for copy, when in sent:
+        if when is None:
+            copy.wait_send()
+        else:
+            pl.when(when)(copy.wait_send)
+
+
+COPIES = 96
+
+
+def in_one_kernel(
+    n_sp,
+    n_tp,
+    tokens,
+    norm_gain,
+    conv_b_w,
+    conv_c_w,
+    conv_x_w,
+    query_w,
+    key_w,
+    value_w,
+    conv_taps,
+    gate_cache,
+    out_conv_w,
+    out_attn_w,
+):
+    rows, width = tokens.shape
+    count = rows * n_tp
+    depth, channels = conv_b_w.shape
+    heads = gate_cache.shape[1]
+    kv_width = key_w.shape[1] + value_w.shape[1]
+    total = gate_cache.shape[0]
+    main_width = (3 * channels + query_w.shape[1]) // n_sp
+    pair_width = (channels + query_w.shape[1]) // n_sp
+    vmem = pl.BlockSpec(memory_space=pltpu.VMEM)
+    hbm = pl.BlockSpec(memory_space=pl.ANY)
+    out_rows = out_conv_w.shape[0] + out_attn_w.shape[0]
+    dma = pltpu.SemaphoreType.DMA
+    mixed, log_rows = pl.pallas_call(
+        functools.partial(layer_kernel, n_sp, n_tp),
+        out_shape=(
+            jax.ShapeDtypeStruct((rows, width), BF16),
+            jax.ShapeDtypeStruct((heads, count), F32),
+        ),
+        in_specs=[vmem] * 10 + [hbm] * 2,
+        out_specs=(vmem, vmem),
+        scratch_shapes=[
+            pltpu.VMEM((total, width), BF16),
+            pltpu.VMEM((total, width), BF16),
+            pltpu.VMEM((n_sp, depth, main_width), BF16),
+            pltpu.VMEM((width, main_width), BF16),
+            pltpu.VMEM((width, kv_width), BF16),
+            pltpu.VMEM((total, LANES), F32),
+            pltpu.VMEM((n_sp, count, pair_width), BF16),
+            pltpu.VMEM((n_sp, count, pair_width), BF16),
+            pltpu.VMEM((n_sp, 8, count), F32),
+            pltpu.VMEM((n_sp, 8, count), F32),
+            pltpu.VMEM((out_rows, width), BF16),
+            pltpu.VMEM((n_tp, rows, width), BF16),
+            pltpu.VMEM((2, rows, width), BF16),
+            pltpu.VMEM((rows, width), BF16),
+            pltpu.VMEM((rows, width), BF16),
+            dma((COPIES,)),
+            dma((n_sp * n_tp,)),
+            dma((2 * n_sp,)),
+            dma((2 * n_sp,)),
+            dma((2 * n_sp,)),
+            dma((12,)),
+            dma((2 * n_sp,)),
+        ],
+        compiler_params=pltpu.CompilerParams(
+            collective_id=0, has_side_effects=True, vmem_limit_bytes=60 * 1024 * 1024
+        ),
+    )(
+        tokens,
+        norm_gain.reshape(1, width),
+        conv_b_w,
+        conv_c_w,
+        conv_x_w,
+        query_w,
+        key_w.T,
+        value_w.T,
+        conv_taps,
+        gate_cache.T,
+        out_conv_w,
+        out_attn_w,
+    )
+    return mixed, log_rows.T
 
 
 def passed_along(value, axis, by):
@@ -193,8 +587,18 @@
         P("tp", None),
         P("tp", None),
     )
+    sizes = dict(mesh.shape)
+
+    def on_one(*args):
+        channels, key_width = args[2].shape[1], args[6].shape[1]
+        grid = (sizes["grp"], sizes["sp"], sizes["tp"])
+        fits = channels == sizes["sp"] * HD and key_width == HD
+        if grid == (2, 4, 4) and fits and args[9].shape[1] == sizes["sp"]:
+            return in_one_kernel(sizes["sp"], sizes["tp"], *args)
+        return on_device(*args)
+
     return jax.shard_map(
-        on_device,
+        on_one,
         mesh=mesh,
         in_specs=placed,
         out_specs=(P(("grp", "sp", "tp"), None), P(("grp", "sp"), "tp")),

time: 186 us -> 77.3 us (0.42)
  waiting for transfers between devices: 74.8 us -> 0 us
  Pallas kernels: 0 us -> 74.2 us
  blocking collectives: 59.7 us -> 0 us
  between operations: 14.3 us -> 0.65 us
  matrix products: 13.3 us -> 0 us
  loops' own time: 9.22 us -> 0 us
  other arithmetic: 4.29 us -> 0 us
  starting transfers between devices: 3.58 us -> 0 us
  local copies, waits for them, and re-layouts: 5.78 us -> 2.27 us
    pallas_call x0 -> x1, Pallas kernels: none -> 74.2 us  [in_one_kernel(): pl.pallas_call(functools.partial(layer_kernel, n_sp, n_tp), out_shape=(ja...]
    all_gather x4 -> x0, blocking collectives: 59.7 us -> none  [the longest x1 15.9 us: on_device(): lax.all_gather(value_w, 'sp', axis=0, tiled=True)]
    all_gather x5 -> x0, waiting for transfers between devices: 47.9 us -> none  [the longest x1 26.8 us: on_device(): lax.all_gather(conv_c_w, 'sp', axis=0, tiled=True)]
    reduce_scatter x1 -> x0, waiting for transfers between devices: 23.8 us -> none  [on_device(): lax.psum_scatter((term + jnp.dot(attn_out, out_attn_w, preferred_element_...]
    dot_general x11 -> x0, matrix products: 13.3 us -> none  [the longest x5 6.21 us: contract_all(): jnp.dot(normed, piece, preferred_element_type=jnp.float32)]
    another operation x5 -> x0, loops' own time: 9.22 us -> none  [the longest x1 5.19 us: on_device(): lax.scan(visit, (fresh(), fresh()), (key_blocks, value_blocks, firsts))]
    slice x9 -> x0, local copies, waits for them, and re-layouts: 3.63 us -> none  [the longest x4 2.58 us: guarded(): return lax.cond(begin <= side[2][half - 1], visit_rows, keep, carry)]
    ppermute x1 -> x0, starting transfers between devices: 3.35 us -> none  [passed_along(): return lax.ppermute(value, axis, pairs)]
  transfers between devices with their start and end apart: 7 -> 0, of which waited for: 5 -> 0; matrix products, arithmetic and copies ran while one was open for 10% -> 0% of each run, Pallas kernels for 0% -> 0%
where the time goes in v2:
time: 77.3 us; the launch traced here: 77.1 us
  Pallas kernels  74.2 us (96%)
  local copies, waits for them, and re-layouts  2.27 us (3%)
    pallas_call x1, Pallas kernels, in_one_kernel(): pl.pallas_call(functools.partial(layer_kernel, n_sp, n_tp), out_shape=(ja...  74.2 us
    unnamed x4, local copies, waits for them, and re-layouts  2.27 us

profile of v2, /device:TPU:0, one launch (start us, length us, event | category | flops | bytes accessed | tf_op | source)
XLA Modules:
  0.0 77.1 jit_solution(4005282187321491316)
XLA Ops:
  0.6 74.2 %shard_map.131 = (bf16[64,2048]{1,0:T(8,128)(2,1)}, f32[4,256]{1,0:T(4,128)}) custom-call(bf16[64,2048]{1,0:T(8,128)(2,1)} %tokens_ref.1, f32[1,2048]{1,0:T(1,128)} %bitcast.8, bf16[512,256]{1,0:T(8,128)(2,1)} %wb_ref.1, bf16[512,256]{1,0:T(8,128)(2,1)} %wc_ref.1, bf16[512,256]{1,0:T(8,128)(2,1)} %wx_ref.1, bf16[512,256]{1,0:T(8,128)(2,1)} %wq_ref.1, ...), custom_call_target="tpu_custom_call" | custom-call | tf_op jit(solution)/shard_map/pallas_call | solution.py:351
  74.8 0.0 copy-start
  74.8 1.7 %copy.16 = bf16[64,2048]{1,0:T(8,128)(2,1)} copy(bf16[64,2048]{1,0:T(8,128)(2,1)} %get-tuple-element.8) | data formatting | bytes 524288
  76.5 0.0 copy-done
  76.5 0.6 copy.17
Async XLA Ops:
  74.8 1.7 %copy-start = (f32[4,256]{1,0:T(4,128)S(1)}, f32[4,256]{1,0:T(4,128)}, u32[]{:S(2)}) copy-start(f32[4,256]{1,0:T(4,128)} %get-tuple-element.5) | copy-start | bytes 12292

commit v3 on v2

--- a/solution.py
+++ b/solution.py
@@ -19,12 +19,12 @@
     n_tp,
     tokens_ref,
     gain_ref,
-    wb_ref,
-    wc_ref,
-    wx_ref,
-    wq_ref,
-    wk_ref,
-    wv_ref,
+    wb_hbm,
+    wc_hbm,
+    wx_hbm,
+    wq_hbm,
+    wk_hbm,
+    wv_hbm,
     taps_ref,
     gate_ref,
     oconv_ref,
@@ -46,6 +46,12 @@
     sib,
     fwd,
     xin,
+    wb_ref,
+    wc_ref,
+    wx_ref,
+    wq_ref,
+    wk_ref,
+    wv_ref,
     send_sem,
     tok_sem,
     main_sem,
@@ -61,12 +67,13 @@
     sibling = t + 1 - 2 * lax.rem(t, 2)
     far = lax.rem(t + 2, n_tp)
     far_sibling = lax.rem(sibling + 2, n_tp)
-    depth = wb_ref.shape[0]
+    depth = wb_hbm.shape[0]
     half = depth // 2
     rows_own, width = tokens_ref.shape
     count = rows_own * n_tp
     total = count * n_sp
-    ch = wb_ref.shape[1] // n_sp
+    sub = rows_own // 2
+    ch = wb_hbm.shape[1] // n_sp
 
     def block(index, size):
         return pl.ds(pl.multiple_of(index * size, size), size)
@@ -81,7 +88,20 @@
                     local_sem.at[2 * d + k],
                 )
             )
-    for copy in local:
+    weights_in = [
+        pltpu.make_async_copy(src, dst, local_sem.at[2 * n_sp + k])
+        for k, (src, dst) in enumerate(
+            (
+                (wb_hbm, wb_ref),
+                (wc_hbm, wc_ref),
+                (wx_hbm, wx_ref),
+                (wq_hbm, wq_ref),
+                (wk_hbm, wk_ref),
+                (wv_hbm, wv_ref),
+            )
+        )
+    ]
+    for copy in weights_in + local:
         copy.start()
 
     barrier = pltpu.get_barrier_semaphore()
@@ -165,15 +185,30 @@
     def kv_rows(z, g_half):
         return wkv.at[block(2 * z + g_half, half)]
 
-    def weights_over(by):
-        z = lax.rem(s + by, n_sp)
-        arrived(main_rows(z, g), main_sem.at[z])
-        send(main_rows(z, g), main_rows(z, g), main_sem.at[n_sp + z], across)
-        arrived(kv_rows(z, g), kv_sem.at[z])
-        send(kv_rows(z, g), kv_rows(z, g), kv_sem.at[n_sp + z], across)
+    def weights_out(h):
+        for step in (1, -1):
+            exists = (s + h < n_sp) if step > 0 else (s >= h)
+            d = lax.rem(s + step * h + n_sp, n_sp)
+            to = {"sp": d}
+            send(kv_rows(s, g), kv_rows(s, g), kv_sem.at[s], to, exists)
+            send(packed.at[d, block(g, half)], main_rows(s, g), main_sem.at[s], to, exists)
+
+    def weights_over(h):
+        for step in (1, -1):
+            exists = (s >= h) if step > 0 else (s + h < n_sp)
+            z = lax.rem(s - step * h + n_sp, n_sp)
+            for rows, sems in ((kv_rows, kv_sem), (main_rows, main_sem)):
+
+                @pl.when(exists)
+                def _(rows=rows, sems=sems, z=z):
+                    arrived(rows(z, g), sems.at[z])
+
+                send(rows(z, g), rows(z, g), sems.at[n_sp + z], across, exists)
 
     tok_spread(tokens_ref, s, 0, None)
     tok[block(s * n_tp + t, rows_own), :] = tokens_ref[...]
+    for copy in weights_in:
+        copy.wait()
     for d in range(n_sp):
         cols = slice(d * ch, (d + 1) * ch)
         packed[d, :, : 2 * ch] = jnp.concatenate([wb_ref[:, cols], wc_ref[:, cols]], axis=1)
@@ -182,17 +217,14 @@
     wkv[block(s, depth), :] = stacked.T.astype(BF16)
     wmain[block(s, depth), :] = packed[s]
 
+    for h in range(1, n_sp):
+        weights_out(h)
     tok_round(1)
-    for by in (2, 1, 3):
-        d = lax.rem(s + by, n_sp)
-        send(packed.at[d, block(g, half)], main_rows(s, g), main_sem.at[s], {"sp": d})
-        send(kv_rows(s, g), kv_rows(s, g), kv_sem.at[s], {"sp": d})
     tok_far(s)
-    tok_round(2)
-    for z_by in (1, 3):
-        weights_over(z_by)
-    tok_round(3)
-    weights_over(2)
+    for h in range(1, n_sp):
+        weights_over(h)
+        if h + 1 < n_sp:
+            tok_round(h + 1)
     for by in (1, 3, 2):
         tok_far(lax.rem(s + by, n_sp))
     for by in range(n_sp):
@@ -261,55 +293,71 @@
         row_sum = jnp.sum(weight, axis=-1, keepdims=True)
         out = jnp.dot(weight.astype(BF16), values[:seen], preferred_element_type=F32)
         attn_out = (out / row_sum).astype(BF16)
-        outs[d] = jnp.concatenate([conv_out[rows], attn_out], axis=1)
+        both_out = jnp.concatenate([conv_out[rows], attn_out], axis=1)
+        for r in range(2):
+            for k in range(n_tp):
+                start = k * rows_own + r * sub
+                outs[r, d, k * sub : (k + 1) * sub] = both_out[start : start + sub]
         logs = jnp.broadcast_to(row_max + jnp.log(row_sum), (count, LANES)).T
         lse_out[d] = logs[: lse_out.shape[1]]
         other = s != d
-        send(outs.at[d], comb.at[s], out_sem.at[s], {"sp": d}, other)
-        send(lse_out.at[d], lse_in.at[s], out_sem.at[n_sp + s], {"sp": d}, other)
-    comb[s] = outs[s]
+        send(outs.at[0, d], comb.at[0, s], out_sem.at[s], {"sp": d}, other)
+    for d in range(n_sp):
+        other = s != d
+        send(outs.at[1, d], comb.at[1, s], out_sem.at[n_sp + s], {"sp": d}, other)
+        send(lse_out.at[d], lse_in.at[s], out_sem.at[2 * n_sp + s], {"sp": d}, other)
+    for r in range(2):
+        comb[r, s] = outs[r, s]
     lse_in[s] = lse_out[s]
     for copy in local:
         copy.wait()
+
+    chunks = 2
+    wide = width // chunks
+
+    def relay(r, c):
+        cols = pl.ds(c * wide, wide)
+        base = 3 * (chunks * r + c)
+        for k in range(2):
+            arrived(sib.at[r, k, :, cols], sum_sem.at[base + k])
+        pair = part[r, far, :, cols].astype(F32) + sib[r, 1, :, cols].astype(F32)
+        fwd[r, :, cols] = pair.astype(BF16)
+        send(fwd.at[r, :, cols], xin.at[r, :, cols], sum_sem.at[base + 2], {"tp": far})
+
+    last = None
+    for r in range(2):
+        for by in range(1, n_sp):
+            z = lax.rem(s + by, n_sp)
+            arrived(comb.at[r, z], out_sem.at[r * n_sp + z])
+        gathered = jnp.concatenate([comb[r, d] for d in range(n_sp)], axis=1)
+        for c in range(chunks):
+            cols = pl.ds(c * wide, wide)
+            term = jnp.dot(gathered, wout[:, cols], preferred_element_type=F32).astype(BF16)
+            for k in range(n_tp):
+                part[r, k, :, cols] = term[k * sub : (k + 1) * sub]
+            for k, owner in ((1, far_sibling), (0, sibling)):
+                send(
+                    part.at[r, owner, :, cols],
+                    sib.at[r, k, :, cols],
+                    sum_sem.at[3 * (chunks * r + c) + k],
+                    {"tp": sibling},
+                )
+            if last is not None:
+                relay(*last)
+            last = (r, c)
+    relay(*last)
     for by in range(1, n_sp):
         z = lax.rem(s + by, n_sp)
-        arrived(comb.at[z], out_sem.at[z])
-        arrived(lse_in.at[z], out_sem.at[n_sp + z])
+        arrived(lse_in.at[z], out_sem.at[2 * n_sp + z])
     for d in range(n_sp):
         lse_ref[d : d + 1, :] = lse_in[d, :1]
-
-    gathered = jnp.concatenate([comb[d] for d in range(n_sp)], axis=1)
-    chunks = 4
-    wide = width // chunks
-
-    def relay(c):
-        cols = pl.ds(c * wide, wide)
-        for k in range(2):
-            arrived(sib.at[k, :, cols], sum_sem.at[3 * c + k])
-        pair = part[far, :, cols].astype(F32) + sib[1, :, cols].astype(F32)
-        fwd[:, cols] = pair.astype(BF16)
-        send(fwd.at[:, cols], xin.at[:, cols], sum_sem.at[3 * c + 2], {"tp": far})
-
-    for c in range(chunks):
-        cols = pl.ds(c * wide, wide)
-        term = jnp.dot(gathered, wout[:, cols], preferred_element_type=F32).astype(BF16)
-        for j in range(n_tp):
-            part[j, :, cols] = term[j * rows_own : (j + 1) * rows_own]
-        for k, owner in ((1, far_sibling), (0, sibling)):
-            send(
-                part.at[owner, :, cols],
-                sib.at[k, :, cols],
-                sum_sem.at[3 * c + k],
-                {"tp": sibling},
-            )
-        if c:
-            relay(c - 1)
-    relay(chunks - 1)
-    for c in range(chunks):
-        cols = pl.ds(c * wide, wide)
-        arrived(xin.at[:, cols], sum_sem.at[3 * c + 2])
-        whole = part[t, :, cols].astype(F32) + sib[0, :, cols].astype(F32)
-        mixed_ref[:, cols] = (whole + xin[:, cols].astype(F32)).astype(BF16)
+    for r in range(2):
+        for c in range(chunks):
+            cols = pl.ds(c * wide, wide)
+            arrived(xin.at[r, :, cols], sum_sem.at[3 * (chunks * r + c) + 2])
+            whole = part[r, t, :, cols].astype(F32) + sib[r, 0, :, cols].astype(F32)
+            whole = whole + xin[r, :, cols].astype(F32)
+            mixed_ref[r * sub : (r + 1) * sub, cols] = whole.astype(BF16)
     for copy, when in sent:
         if when is None:
             copy.wait_send()
@@ -317,7 +365,7 @@
             pl.when(when)(copy.wait_send)
 
 
-COPIES = 96
+COPIES = 128
 
 
 def in_one_kernel(
@@ -354,7 +402,7 @@
             jax.ShapeDtypeStruct((rows, width), BF16),
             jax.ShapeDtypeStruct((heads, count), F32),
         ),
-        in_specs=[vmem] * 10 + [hbm] * 2,
+        in_specs=[vmem] * 2 + [hbm] * 6 + [vmem] * 2 + [hbm] * 2,
         out_specs=(vmem, vmem),
         scratch_shapes=[
             pltpu.VMEM((total, width), BF16),
@@ -363,22 +411,28 @@
             pltpu.VMEM((width, main_width), BF16),
             pltpu.VMEM((width, kv_width), BF16),
             pltpu.VMEM((total, LANES), F32),
-            pltpu.VMEM((n_sp, count, pair_width), BF16),
-            pltpu.VMEM((n_sp, count, pair_width), BF16),
+            pltpu.VMEM((2, n_sp, count // 2, pair_width), BF16),
+            pltpu.VMEM((2, n_sp, count // 2, pair_width), BF16),
             pltpu.VMEM((n_sp, 8, count), F32),
             pltpu.VMEM((n_sp, 8, count), F32),
             pltpu.VMEM((out_rows, width), BF16),
-            pltpu.VMEM((n_tp, rows, width), BF16),
-            pltpu.VMEM((2, rows, width), BF16),
-            pltpu.VMEM((rows, width), BF16),
-            pltpu.VMEM((rows, width), BF16),
+            pltpu.VMEM((2, n_tp, rows // 2, width), BF16),
+            pltpu.VMEM((2, 2, rows // 2, width), BF16),
+            pltpu.VMEM((2, rows // 2, width), BF16),
+            pltpu.VMEM((2, rows // 2, width), BF16),
+            pltpu.VMEM(conv_b_w.shape, BF16),
+            pltpu.VMEM(conv_c_w.shape, BF16),
+            pltpu.VMEM(conv_x_w.shape, BF16),
+            pltpu.VMEM(query_w.shape, BF16),
+            pltpu.VMEM(key_w.shape[::-1], BF16),
+            pltpu.VMEM(value_w.shape[::-1], BF16),
             dma((COPIES,)),
             dma((n_sp * n_tp,)),
             dma((2 * n_sp,)),
             dma((2 * n_sp,)),
-            dma((2 * n_sp,)),
+            dma((3 * n_sp,)),
             dma((12,)),
-            dma((2 * n_sp,)),
+            dma((2 * n_sp + 6,)),
         ],
         compiler_params=pltpu.CompilerParams(
             collective_id=0, has_side_effects=True, vmem_limit_bytes=60 * 1024 * 1024

time: 77.3 us -> 75.3 us (0.974)
  Pallas kernels: 74.2 us -> 72.2 us
    pallas_call x1, Pallas kernels: 74.2 us -> 72.2 us  [in_one_kernel(): pl.pallas_call(functools.partial(layer_kernel, n_sp, n_tp), out_shape=(ja...]
where the time goes in v3:
time: 75.3 us; the launch traced here: 75.2 us
  Pallas kernels  72.2 us (96%)
  local copies, waits for them, and re-layouts  2.27 us (3%)
    pallas_call x1, Pallas kernels, in_one_kernel(): pl.pallas_call(functools.partial(layer_kernel, n_sp, n_tp), out_shape=(ja...  72.2 us
    unnamed x4, local copies, waits for them, and re-layouts  2.27 us

profile of v3, /device:TPU:0, one launch (start us, length us, event | category | flops | bytes accessed | tf_op | source)
XLA Modules:
  0.0 75.2 jit_solution(13883860430657803386)
XLA Ops:
  0.6 72.2 %shard_map.131 = (bf16[64,2048]{1,0:T(8,128)(2,1)}, f32[4,256]{1,0:T(4,128)}) custom-call(bf16[64,2048]{1,0:T(8,128)(2,1)} %tokens_ref.1, f32[1,2048]{1,0:T(1,128)} %bitcast.8, bf16[512,256]{1,0:T(8,128)(2,1)} %wb_hbm.1, bf16[512,256]{1,0:T(8,128)(2,1)} %wc_hbm.1, bf16[512,256]{1,0:T(8,128)(2,1)} %wx_hbm.1, bf16[512,256]{1,0:T(8,128)(2,1)} %wq_hbm.1, ...), custom_call_target="tpu_custom_call" | custom-call | tf_op jit(solution)/shard_map/pallas_call | solution.py:399
  72.9 0.0 copy-start
  72.9 1.7 %copy.16 = bf16[64,2048]{1,0:T(8,128)(2,1)} copy(bf16[64,2048]{1,0:T(8,128)(2,1)} %get-tuple-element.8) | data formatting | bytes 524288
  74.6 0.0 copy-done
  74.6 0.6 copy.17
Async XLA Ops:
  72.9 1.7 %copy-start = (f32[4,256]{1,0:T(4,128)S(1)}, f32[4,256]{1,0:T(4,128)}, u32[]{:S(2)}) copy-start(f32[4,256]{1,0:T(4,128)} %get-tuple-element.5) | copy-start | bytes 12292

commit v4 on v3

--- a/solution.py
+++ b/solution.py
@@ -174,10 +174,19 @@
 
             tok_spread(tok_block(z, t), z, step, exists)
 
-    def tok_far(z):
+    def tok_far(z, when=None):
         arrival = tok_sem.at[z * n_tp + far]
-        arrived(tok_block(z, far), arrival)
-        send(tok_block(z, far), tok_block(z, far), arrival, {"tp": sibling})
+
+        @pl.when(True if when is None else when)
+        def _():
+            arrived(tok_block(z, far), arrival)
+
+        send(tok_block(z, far), tok_block(z, far), arrival, {"tp": sibling}, when)
+
+    def far_round(h):
+        for step in (1, -1):
+            exists = (s >= h) if step > 0 else (s + h < n_sp)
+            tok_far(lax.rem(s - step * h + n_sp, n_sp), exists)
 
     def main_rows(z, g_half):
         return wmain.at[block(2 * z + g_half, half)]
@@ -217,16 +226,16 @@
     wkv[block(s, depth), :] = stacked.T.astype(BF16)
     wmain[block(s, depth), :] = packed[s]
 
+    tok_round(1)
     for h in range(1, n_sp):
         weights_out(h)
-    tok_round(1)
     tok_far(s)
-    for h in range(1, n_sp):
-        weights_over(h)
-        if h + 1 < n_sp:
-            tok_round(h + 1)
-    for by in (1, 3, 2):
-        tok_far(lax.rem(s + by, n_sp))
+    for h in range(2, n_sp):
+        tok_round(h)
+        far_round(h - 1)
+        weights_over(h - 1)
+    weights_over(n_sp - 1)
+    far_round(n_sp - 1)
     for by in range(n_sp):
         z = lax.rem(s + by, n_sp)
         arrived(tok_block(z, sibling), tok_sem.at[z * n_tp + sibling])

time: 75.3 us -> 71.3 us (0.947)
  Pallas kernels: 72.2 us -> 68.2 us
    pallas_call x1, Pallas kernels: 72.2 us -> 68.2 us  [in_one_kernel(): pl.pallas_call(functools.partial(layer_kernel, n_sp, n_tp), out_shape=(ja...]
where the time goes in v4:
time: 71.3 us; the launch traced here: 71.1 us
  Pallas kernels  68.2 us (96%)
  local copies, waits for them, and re-layouts  2.27 us (3%)
    pallas_call x1, Pallas kernels, in_one_kernel(): pl.pallas_call(functools.partial(layer_kernel, n_sp, n_tp), out_shape=(ja...  68.2 us
    unnamed x4, local copies, waits for them, and re-layouts  2.27 us

profile of v4, /device:TPU:0, one launch (start us, length us, event | category | flops | bytes accessed | tf_op | source)
XLA Modules:
  0.0 71.1 jit_solution(8896712449543679080)
XLA Ops:
  0.6 68.2 %shard_map.131 = (bf16[64,2048]{1,0:T(8,128)(2,1)}, f32[4,256]{1,0:T(4,128)}) custom-call(bf16[64,2048]{1,0:T(8,128)(2,1)} %tokens_ref.1, f32[1,2048]{1,0:T(1,128)} %bitcast.8, bf16[512,256]{1,0:T(8,128)(2,1)} %wb_hbm.1, bf16[512,256]{1,0:T(8,128)(2,1)} %wc_hbm.1, bf16[512,256]{1,0:T(8,128)(2,1)} %wx_hbm.1, bf16[512,256]{1,0:T(8,128)(2,1)} %wq_hbm.1, ...), custom_call_target="tpu_custom_call" | custom-call | tf_op jit(solution)/shard_map/pallas_call | solution.py:408
  68.9 0.0 copy-start
  68.9 1.7 %copy.16 = bf16[64,2048]{1,0:T(8,128)(2,1)} copy(bf16[64,2048]{1,0:T(8,128)(2,1)} %get-tuple-element.8) | data formatting | bytes 524288
  70.5 0.0 copy-done
  70.5 0.6 copy.17
Async XLA Ops:
  68.9 1.7 %copy-start = (f32[4,256]{1,0:T(4,128)S(1)}, f32[4,256]{1,0:T(4,128)}, u32[]{:S(2)}) copy-start(f32[4,256]{1,0:T(4,128)} %get-tuple-element.5) | copy-start | bytes 12292

commit v5 on v4

--- a/solution.py
+++ b/solution.py
@@ -150,12 +150,15 @@
     def both(a, b):
         return b if a is None else jnp.logical_and(a, b)
 
-    def tok_block(z, x):
-        return tok.at[block(z * n_tp + x, rows_own)]
-
-    def tok_spread(src, z, step, when):
-        arrival = tok_sem.at[z * n_tp + t]
-        dst = tok_block(z, t)
+    def tok_block(z, x, p):
+        return tok.at[block((z * n_tp + x) * 2 + p, sub)]
+
+    def tok_arrival(z, x, p):
+        return tok_sem.at[(z * n_tp + x) * 2 + p]
+
+    def tok_spread(src, z, p, step, when):
+        arrival = tok_arrival(z, t, p)
+        dst = tok_block(z, t, p)
         if step >= 0:
             send(src, dst, arrival, {"sp": lax.rem(s + 1, n_sp)}, both(when, s < n_sp - 1))
         if step <= 0:
@@ -164,24 +167,27 @@
         send(src, dst, arrival, {"tp": sibling}, when)
 
     def tok_round(h):
-        for step in (1, -1):
-            z = lax.rem(s - step * h + n_sp, n_sp)
-            exists = (s >= h) if step > 0 else (s + h < n_sp)
-
-            @pl.when(exists)
-            def _(z=z):
-                arrived(tok_block(z, t), tok_sem.at[z * n_tp + t])
-
-            tok_spread(tok_block(z, t), z, step, exists)
+        for p in range(2):
+            for step in (1, -1):
+                z = lax.rem(s - step * h + n_sp, n_sp)
+                exists = (s >= h) if step > 0 else (s + h < n_sp)
+
+                @pl.when(exists)
+                def _(z=z):
+                    arrived(tok_block(z, t, p), tok_arrival(z, t, p))
+
+                tok_spread(tok_block(z, t, p), z, p, step, exists)
 
     def tok_far(z, when=None):
-        arrival = tok_sem.at[z * n_tp + far]
-
-        @pl.when(True if when is None else when)
-        def _():
-            arrived(tok_block(z, far), arrival)
-
-        send(tok_block(z, far), tok_block(z, far), arrival, {"tp": sibling}, when)
+        for p in range(2):
+            arrival = tok_arrival(z, far, p)
+            here = tok_block(z, far, p)
+
+            @pl.when(True if when is None else when)
+            def _():
+                arrived(here, arrival)
+
+            send(here, here, arrival, {"tp": sibling}, when)
 
     def far_round(h):
         for step in (1, -1):
@@ -214,7 +220,8 @@
 
                 send(rows(z, g), rows(z, g), sems.at[n_sp + z], across, exists)
 
-    tok_spread(tokens_ref, s, 0, None)
+    for p in range(2):
+        tok_spread(tokens_ref.at[pl.ds(p * sub, sub)], s, p, 0, None)
     tok[block(s * n_tp + t, rows_own), :] = tokens_ref[...]
     for copy in weights_in:
         copy.wait()
@@ -238,8 +245,9 @@
     far_round(n_sp - 1)
     for by in range(n_sp):
         z = lax.rem(s + by, n_sp)
-        arrived(tok_block(z, sibling), tok_sem.at[z * n_tp + sibling])
-        arrived(tok_block(z, far_sibling), tok_sem.at[z * n_tp + far_sibling])
+        for p in range(2):
+            for x in (sibling, far_sibling):
+                arrived(tok_block(z, x, p), tok_arrival(z, x, p))
 
     def normalize(i, unused):
         rows = block(i, rows_own)
@@ -374,7 +382,7 @@
             pl.when(when)(copy.wait_send)
 
 
-COPIES = 128
+COPIES = 192
 
 
 def in_one_kernel(
@@ -436,7 +444,7 @@
             pltpu.VMEM(key_w.shape[::-1], BF16),
             pltpu.VMEM(value_w.shape[::-1], BF16),
             dma((COPIES,)),
-            dma((n_sp * n_tp,)),
+            dma((2 * n_sp * n_tp,)),
             dma((2 * n_sp,)),
             dma((2 * n_sp,)),
             dma((3 * n_sp,)),

time: 71.3 us -> 69.8 us (0.979)
  Pallas kernels: 68.2 us -> 66.7 us
    pallas_call x1, Pallas kernels: 68.2 us -> 66.7 us  [in_one_kernel(): pl.pallas_call(functools.partial(layer_kernel, n_sp, n_tp), out_shape=(ja...]
where the time goes in v5:
time: 69.8 us; the launch traced here: 69.6 us
  Pallas kernels  66.7 us (96%)
  local copies, waits for them, and re-layouts  2.27 us (3%)
    pallas_call x1, Pallas kernels, in_one_kernel(): pl.pallas_call(functools.partial(layer_kernel, n_sp, n_tp), out_shape=(ja...  66.7 us
    unnamed x4, local copies, waits for them, and re-layouts  2.27 us

profile of v5, /device:TPU:0, one launch (start us, length us, event | category | flops | bytes accessed | tf_op | source)
XLA Modules:
  0.0 69.6 jit_solution(2735218189843818345)
XLA Ops:
  0.6 66.7 %shard_map.131 = (bf16[64,2048]{1,0:T(8,128)(2,1)}, f32[4,256]{1,0:T(4,128)}) custom-call(bf16[64,2048]{1,0:T(8,128)(2,1)} %tokens_ref.1, f32[1,2048]{1,0:T(1,128)} %bitcast.8, bf16[512,256]{1,0:T(8,128)(2,1)} %wb_hbm.1, bf16[512,256]{1,0:T(8,128)(2,1)} %wc_hbm.1, bf16[512,256]{1,0:T(8,128)(2,1)} %wx_hbm.1, bf16[512,256]{1,0:T(8,128)(2,1)} %wq_hbm.1, ...), custom_call_target="tpu_custom_call" | custom-call | tf_op jit(solution)/shard_map/pallas_call | solution.py:416
  67.3 0.0 copy-start
  67.3 1.7 %copy.16 = bf16[64,2048]{1,0:T(8,128)(2,1)} copy(bf16[64,2048]{1,0:T(8,128)(2,1)} %get-tuple-element.8) | data formatting | bytes 524288
  69.0 0.0 copy-done
  69.0 0.6 copy.17
Async XLA Ops:
  67.3 1.7 %copy-start = (f32[4,256]{1,0:T(4,128)S(1)}, f32[4,256]{1,0:T(4,128)}, u32[]{:S(2)}) copy-start(f32[4,256]{1,0:T(4,128)} %get-tuple-element.5) | copy-start | bytes 12292
